TPU v7x, 32 devices: a whole 2x2x4 slice. The times are simulated.
32 devices in a mesh: fs: 4 (over z), rep: 4 (over y, x), tp: 2 (over core).
Axes of the slice: x: 2, y: 2, z: 4, core: 2. Of those that a mesh axis runs over, the one named last changes fastest.
Arguments:
- normed: bfloat16 [10240, 2048], P(('fs', 'rep')), may hold values from -150 to 150
- rec_cot: bfloat16 [10240, 2048], P(('fs', 'rep'), 'tp'), may hold values from -1.4823177 to 1.4823177
- conv_out: bfloat16 [10240, 2048], P(('fs', 'rep'), 'tp'), may hold values from -6 to 6
- gate_cot: bfloat16 [10240, 2048], P(('fs', 'rep'), 'tp'), may hold values from -0.05908203 to 0.05908203
- rec_weight: float32 [2048, 2048], P('fs', 'tp'), may hold values from -0.125 to 0.125
- rec_moment: float32 [2048, 2048], P('fs', 'tp'), may hold values from -6 to 6
- rec_right: bfloat16 [2048, 256], P('tp'), may hold values from -1 to 2
- gate_weight: float32 [8, 256, 256], P('tp', 'fs'), may hold values from -0.375 to 0.375
- gate_moment: float32 [8, 256, 256], P('tp', 'fs'), may hold values from -6 to 6
- gate_left: bfloat16 [8, 256, 256], P('tp', 'fs'), may hold values from -1 to 2
- gate_right: bfloat16 [8, 256, 256], P('tp'), may hold values from -1 to 2
Outputs:
- rec_weight_new: float32 [2048, 2048], P('fs', 'tp')
- rec_moment_new: float32 [2048, 2048], P('fs', 'tp')
- rec_step: float32 [2048, 2048], P('fs', 'tp')
- rec_copy: bfloat16 [2048, 2048], P('fs', 'tp')
- gate_weight_new: float32 [8, 256, 256], P('tp', 'fs')
- gate_moment_new: float32 [8, 256, 256], P('tp', 'fs')
- gate_step: float32 [8, 256, 256], P('tp', 'fs')
- gate_copy: bfloat16 [8, 256, 256], P('tp', 'fs')
All inputs are finite; a program needn't handle non-finite values.
Results may differ from a plain program's by a relative error of at most 0.001.
Values sent between devices are 32-bit elements; how exact they have to be, the bound alone decides.
A program may use at most 64 MiB of HBM per device.

v0:
```python
import jax
import jax.numpy as jnp
from jax import lax
from jax.sharding import PartitionSpec as P

BETA = 0.9
LEARN_RATE = 0.02
EPSILON = 1e-06


def precondition_right(gradient, factor):
    row_count = gradient.shape[0]
    block_size = factor.shape[1]
    blocks = factor.shape[0] // block_size
    shaped = gradient.reshape(row_count, blocks, block_size)
    factors = factor.astype(jnp.float32).reshape(blocks, block_size, block_size)
    result = jnp.einsum("rbi,bij->rbj", shaped, factors, precision=lax.Precision.HIGHEST)
    return result.reshape(row_count, blocks * block_size)


def shards(
    normed,
    rec_cot,
    conv_out,
    gate_cot,
    rec_weight,
    rec_moment,
    rec_right,
    gate_weight,
    gate_moment,
    gate_left,
    gate_right,
):
    token_count = normed.shape[0]
    columns = normed
    partial_rows = lax.psum_scatter(
        lax.dot_general(
            columns, rec_cot, (((0,), (0,)), ((), ())), preferred_element_type=jnp.float32
        ),
        "fs",
        scatter_dimension=0,
        tiled=True,
    )
    rec_grad = lax.psum(partial_rows, "rep")
    rec_pre = precondition_right(rec_grad, rec_right)
    block_count, own_rows, block_size = gate_weight.shape
    conv_blocks = conv_out.reshape(token_count, block_count, block_size)
    cot_blocks = gate_cot.reshape(token_count, block_count, block_size)
    gate_term = jnp.einsum(
        "tbi,tbj->bij", conv_blocks, cot_blocks, preferred_element_type=jnp.float32
    )
    right_factor = gate_right.astype(jnp.float32)
    left_factor = gate_left.astype(jnp.float32)
    part_grad = lax.psum_scatter(gate_term, "fs", scatter_dimension=1, tiled=True)
    gate_grad = lax.psum(part_grad, "rep")
    right_done = jnp.einsum(
        "bij,bjk->bik", gate_grad, right_factor, precision=lax.Precision.HIGHEST
    )
    columns = left_factor
    gate_pre = jnp.einsum(
        "bri,bik->brk",
        columns,
        lax.all_gather(right_done, "fs", axis=1, tiled=True),
        precision=lax.Precision.HIGHEST,
    )
    rec_moment_new = BETA * rec_moment + rec_pre
    gate_moment_new = BETA * gate_moment + gate_pre
    totals = lax.psum(
        (
            jnp.sum(rec_grad * rec_grad),
            jnp.sum(rec_moment_new * rec_moment_new),
            jnp.sum(gate_grad * gate_grad),
            jnp.sum(gate_moment_new * gate_moment_new),
        ),
        ("fs", "tp"),
    )
    rec_scale = jnp.sqrt(totals[0]) / jnp.sqrt(totals[1] + EPSILON)
    gate_scale = jnp.sqrt(totals[2]) / jnp.sqrt(totals[3] + EPSILON)
    rec_taken = LEARN_RATE * rec_scale * rec_moment_new
    gate_taken = LEARN_RATE * gate_scale * gate_moment_new
    rec_new = rec_weight - rec_taken
    gate_new = gate_weight - gate_taken
    return (
        rec_new,
        rec_moment_new,
        rec_taken,
        rec_new.astype(jnp.bfloat16),
        gate_new,
        gate_moment_new,
        gate_taken,
        gate_new.astype(jnp.bfloat16),
    )


def solution(mesh):
    in_specs = (
        P(("fs", "rep"), None),
        P(("fs", "rep"), "tp"),
        P(("fs", "rep"), "tp"),
        P(("fs", "rep"), "tp"),
        P("fs", "tp"),
        P("fs", "tp"),
        P("tp", None),
        P("tp", "fs", None),
        P("tp", "fs", None),
        P("tp", "fs", None),
        P("tp", None, None),
    )
    out_specs = (
        P("fs", "tp"),
        P("fs", "tp"),
        P("fs", "tp"),
        P("fs", "tp"),
        P("tp", "fs", None),
        P("tp", "fs", None),
        P("tp", "fs", None),
        P("tp", "fs", None),
    )
    return jax.shard_map(shards, mesh=mesh, in_specs=in_specs, out_specs=out_specs, check_vma=False)
```

profile of v0, /device:TPU:0, one launch (start us, length us, event | category | flops | bytes accessed | tf_op | source)
XLA Modules:
  0.0 330.2 jit_solution(16885048392378607039)
XLA Ops:
  7.2 0.0 copy-start
  7.2 0.0 reduce-scatter.5.cloned.1.call-start
  7.2 2.6 copy.25
  9.8 3.3 fusion.3
  13.1 0.0 reduce-scatter.5.cloned.1.call-update
  13.1 0.0 reduce-scatter.3.cloned.1.call-start
  13.1 0.0 copy-done
  13.1 7.0 %fusion.9 = f32[2048,1024]{1,0:T(8,128)} fusion(bf16[640,2048]{1,0:T(8,128)(2,1)S(1)} %copy-done, bf16[640,1024]{1,0:T(8,128)(2,1)} %param.12), kind=kOutput, calls=%fused_computation.17 | convolution fusion | flops 2684354560 | bytes 12320768 | tf_op jit(solution)/shard_map/dot_general | solution.py:37
  20.1 0.0 reduce-scatter.3.cloned.1.call-update
  20.2 0.0 copy-start.3
  20.2 0.0 all-reduce.4.cloned.1.call-start
  20.2 23.0 %reduce-scatter.5.cloned.1.call-done = f32[4,64,256]{2,1,0:T(8,128)} async-done(((f32[4,256,256]{2,1,0:T(8,128)}), f32[4,64,256]{2,1,0:T(8,128)}) %reduce-scatter.5.cloned.1.call-update) | async-done | bytes 262160 | tf_op jit(solution)/shard_map/reduce_scatter | solution.py:54
  43.2 145.5 %reduce-scatter.3.cloned.1.call-done = f32[512,1024]{1,0:T(8,128)} async-done(((f32[2048,1024]{1,0:T(8,128)}), f32[512,1024]{1,0:T(8,128)}) %reduce-scatter.3.cloned.1.call-update) | async-done | bytes 2097168 | tf_op jit(solution)/shard_map/reduce_scatter | solution.py:36
  188.8 0.0 all-reduce.4.cloned.1.call-update
  188.8 0.0 all-gather.2.cloned.1.call-start
  188.8 77.6 %all-reduce.4.cloned.1.call-done = (f32[512,1024]{1,0:T(8,128)}, f32[4,64,256]{2,1,0:T(8,128)}) async-done(((f32[512,1024]{1,0:T(8,128)}, f32[4,64,256]{2,1,0:T(8,128)}), (f32[512,1024]{1,0:T(8,128)}, f32[4,64,256]{2,1,0:T(8,128)})) %all-reduce.4.cloned.1.call-update) | async-done | bytes 2359312 | tf_op jit(solution)/shard_map/psum | solution.py:44
  266.5 2.2 fusion.10
  268.7 0.0 all-gather.2.cloned.1.call-update
  268.7 0.0 copy-done.3
  268.7 4.1 %fusion = f32[4,512,256]{1,2,0:T(8,128)} fusion(bf16[4,256,256]{2,1,0:T(8,128)(2,1)S(1)} %bitcast.29, f32[64,4,8,256]{3,2,1,0:T(8,128)} %bitcast.25), kind=kOutput, calls=%fused_computation | convolution fusion | flops 1610612736 | bytes 4718592 | tf_op jit(solution)/shard_map/rbi,bij->rbj/dot_general | solution.py:17
  272.8 0.0 copy-start.2
  272.8 2.9 copy.21
  275.8 0.0 copy-done.2
  275.8 0.7 multiply_reduce_fusion.3
  276.4 0.0 copy-start.4
  276.4 0.0 copy-start.6
  276.4 5.7 %multiply_reduce_fusion = (f32[]{:T(128)}, f32[512,1024]{1,0:T(8,128)}, f32[]{:T(128)}) fusion(f32[512,1024]{1,0:T(8,128)} %copy.21, f32[512,1024]{1,0:T(8,128)} %param.16, f32[512,1024]{1,0:T(8,128)} %get-tuple-element.12), kind=kLoop, calls=%fused_computation.3 | loop fusion | flops 3145726 | bytes 8388616 | tf_op jit(solution)/shard_map/reduce_sum | solution.py:71
  282.1 14.7 %all-gather.2.cloned.1.call-done = f32[4,256,256]{2,1,0:T(8,128)} async-done(((f32[4,64,256]{2,1,0:T(8,128)}), f32[4,256,256]{2,1,0:T(8,128)}) %all-gather.2.cloned.1.call-update) | async-done | bytes 1048592 | tf_op jit(solution)/shard_map/all_gather | solution.py:63
  296.8 0.0 copy-done.4
  296.8 0.0 copy-done.6
  296.8 2.4 multiply_reduce_fusion.2
  299.2 0.0 copy-start.1
  299.2 15.3 %all-reduce = (f32[]{:T(128)}, f32[]{:T(128)}, f32[]{:T(128)}, f32[]{:T(128)}) all-reduce(f32[]{:T(128)} %get-tuple-element.24, f32[]{:T(128)} %get-tuple-element.20, f32[]{:T(128)} %multiply_reduce_fusion.3, f32[]{:T(128)} %get-tuple-element.22), channel_id=1, replica_groups=mesh['fs'=4,'rep'=4,'tp'=2] {'fs','tp'}, use_global_device_ids=true, to_apply=%region_3.0 | all-reduce | flops 4 | bytes 32 | tf_op jit(solution)/shard_map/psum | solution.py:68
  317.3 0.0 copy-start.5
  317.3 5.5 %fusion.8 = (bf16[512,1024]{1,0:T(8,128)(2,1)}, f32[512,1024]{1,0:T(8,128)}, f32[512,1024]{1,0:T(8,128)}) fusion(f32[512,1024]{1,0:T(8,128)} %param.15, f32[512,1024]{1,0:T(8,128)} %get-tuple-element.21, f32[]{:T(128)S(6)} %mul.46), kind=kLoop, calls=%fused_computation.16 | loop fusion | flops 1572864 | bytes 9437188 | tf_op jit(solution)/shard_map/convert_element_type | solution.py:87
  322.8 0.0 copy-done.1
  322.8 0.0 copy-done.5
  322.8 0.9 fusion.7
Async XLA Ops:
  7.2 6.0 %copy-start = (bf16[640,2048]{1,0:T(8,128)(2,1)S(1)}, bf16[640,2048]{1,0:T(8,128)(2,1)}, u32[]{:S(2)}) copy-start(bf16[640,2048]{1,0:T(8,128)(2,1)} %param.11) | copy-start | bytes 7864324
  7.2 36.1 %reduce-scatter.5.cloned.1.call-start = ((), (), s32[]{:S(2)}) async-start(), calls=%async_computation.3 | async-start | bytes 1310720 | tf_op jit(solution)/shard_map/reduce_scatter | solution.py:54
  13.1 175.7 %reduce-scatter.3.cloned.1.call-start = ((), (), s32[]{:S(2)}) async-start(), calls=%async_computation.2 | async-start | bytes 10485760 | tf_op jit(solution)/shard_map/reduce_scatter | solution.py:36
  20.2 248.5 %copy-start.3 = (bf16[1024,256]{1,0:T(8,128)(2,1)S(1)}, bf16[1024,256]{1,0:T(8,128)(2,1)}, u32[]{:S(2)}) copy-start(bf16[1024,256]{1,0:T(8,128)(2,1)} %param.17) | copy-start | bytes 1572868
  20.2 246.3 %all-reduce.4.cloned.1.call-start = ((), (), s32[]{:S(2)}) async-start(), calls=%async_computation.5 | async-start | bytes 4718592 | tf_op jit(solution)/shard_map/psum | solution.py:44
  188.8 108.1 %all-gather.2.cloned.1.call-start = ((), (), s32[]{:S(2)}) async-start(), calls=%async_computation.4 | async-start | bytes 1310720 | tf_op jit(solution)/shard_map/all_gather | solution.py:63
  272.8 2.9 copy-start.2
  276.4 20.4 %copy-start.4 = (f32[4,64,256]{2,1,0:T(8,128)S(1)}, f32[4,64,256]{2,1,0:T(8,128)}, u32[]{:S(2)}) copy-start(f32[4,64,256]{2,1,0:T(8,128)} %param.19) | copy-start | bytes 786436
  276.4 20.4 %copy-start.6 = (bf16[4,64,256]{2,1,0:T(8,128)(2,1)S(1)}, bf16[4,64,256]{2,1,0:T(8,128)(2,1)}, u32[]{:S(2)}) copy-start(bf16[4,64,256]{2,1,0:T(8,128)(2,1)} %param.20) | copy-start | bytes 393220
  299.2 23.6 %copy-start.1 = (f32[4,64,256]{2,1,0:T(8,128)}, f32[4,64,256]{2,1,0:T(8,128)S(1)}, u32[]{:S(2)}) copy-start(f32[4,64,256]{2,1,0:T(8,128)S(1)} %get-tuple-element.23) | copy-start | bytes 786436
  317.3 5.5 %copy-start.5 = (f32[4,64,256]{2,1,0:T(8,128)S(1)}, f32[4,64,256]{2,1,0:T(8,128)}, u32[]{:S(2)}) copy-start(f32[4,64,256]{2,1,0:T(8,128)} %param.18) | copy-start | bytes 786436
Sparse Core Ops, SparseCore 0:
  13.2 29.9 reduce-scatter.4
  45.6 143.1 reduce-scatter.2
  191.9 74.4 all-reduce.3
  268.8 27.9 all-gather.1
where the time goes:
time: 331 us; the launch traced here: 330 us
  waiting for transfers between devices  261 us (79%)
  matrix products  19 us (6%)
  between operations  16.6 us (5%)
  blocking collectives  15.3 us (5%)
  other arithmetic  12.7 us (4%)
  local copies, waits for them, and re-layouts  5.54 us (2%)
    reduce_scatter x1, waiting for transfers between devices, shards(): lax.psum_scatter(lax.dot_general(columns, rec_cot, (((0,), (0,)), ((), ()...  146 us
    psum x1, waiting for transfers between devices, shards(): rec_grad = lax.psum(partial_rows, 'rep')  77.6 us
    reduce_scatter x1, waiting for transfers between devices, shards(): lax.psum_scatter(gate_term, 'fs', scatter_dimension=1, tiled=True)  23 us
    psum x1, blocking collectives, shards(): lax.psum((jnp.sum(rec_grad * rec_grad), jnp.sum(rec_moment_new * rec_mome...  15.3 us
    all_gather x1, waiting for transfers between devices, shards(): lax.all_gather(right_done, 'fs', axis=1, tiled=True)  14.7 us
    dot_general x1, matrix products, shards(): lax.dot_general(columns, rec_cot, (((0,), (0,)), ((), ())), preferred_ele...  7 us
  transfers between devices with their start and end apart: 4, of which 4 were waited for; matrix products, arithmetic and copies ran while one was open for 6% of the time, Pallas kernels for 0%

commit v1 on v0

--- a/solution.py
+++ b/solution.py
@@ -6,6 +6,12 @@
 BETA = 0.9
 LEARN_RATE = 0.02
 EPSILON = 1e-06
+
+
+def summed_here(shard, axis):
+    pieces = lax.all_gather(shard, axis, axis=0, tiled=False)
+    result = pieces.sum(axis=0)
+    return result
 
 
 def precondition_right(gradient, factor):
@@ -41,7 +47,7 @@
         scatter_dimension=0,
         tiled=True,
     )
-    rec_grad = lax.psum(partial_rows, "rep")
+    rec_grad = summed_here(partial_rows, "rep")
     rec_pre = precondition_right(rec_grad, rec_right)
     block_count, own_rows, block_size = gate_weight.shape
     conv_blocks = conv_out.reshape(token_count, block_count, block_size)

time: 331 us -> 408 us (1.23)
  waiting for transfers between devices: 261 us -> 328 us
  other arithmetic: 12.7 us -> 18.5 us
    all_gather x0 -> x1, waiting for transfers between devices: none -> 86.2 us  [summed_here(): pieces = lax.all_gather(shard, axis, axis=0, tiled=False)]
    psum x1, waiting for transfers between devices: 77.6 us -> 37.4 us  [shards(): gate_grad = lax.psum(part_grad, 'rep')]
    all_gather x1, waiting for transfers between devices: 14.7 us -> 29.9 us  [shards(): lax.all_gather(right_done, 'fs', axis=1, tiled=True)]
    reduce_scatter x1, waiting for transfers between devices: 23 us -> 30.1 us  [shards(): lax.psum_scatter(gate_term, 'fs', scatter_dimension=1, tiled=True)]
    reduce_sum x0 -> x1, other arithmetic: none -> 5.88 us  [summed_here(): result = pieces.sum(axis=0)]
  transfers between devices with their start and end apart: 4 -> 5, of which waited for: 4 -> 5; matrix products, arithmetic and copies ran while one was open for 6% -> 3% of each run, Pallas kernels for 0% -> 0%
where the time goes in v1:
time: 408 us
  waiting for transfers between devices  328 us (80%)
  matrix products  18.9 us (5%)
  other arithmetic  18.5 us (5%)
  blocking collectives  16.8 us (4%)
  between operations  16.6 us (4%)
  local copies, waits for them, and re-layouts  8.43 us (2%)
    reduce_scatter x1, waiting for transfers between devices, shards(): lax.psum_scatter(lax.dot_general(columns, rec_cot, (((0,), (0,)), ((), ()...  145 us
    all_gather x1, waiting for transfers between devices, summed_here(): pieces = lax.all_gather(shard, axis, axis=0, tiled=False)  86.2 us
    psum x1, waiting for transfers between devices, shards(): gate_grad = lax.psum(part_grad, 'rep')  37.4 us
    reduce_scatter x1, waiting for transfers between devices, shards(): lax.psum_scatter(gate_term, 'fs', scatter_dimension=1, tiled=True)  30.1 us
    all_gather x1, waiting for transfers between devices, shards(): lax.all_gather(right_done, 'fs', axis=1, tiled=True)  29.9 us
    psum x1, blocking collectives, shards(): lax.psum((jnp.sum(rec_grad * rec_grad), jnp.sum(rec_moment_new * rec_mome...  16.8 us
  transfers between devices with their start and end apart: 5, of which 5 were waited for; matrix products, arithmetic and copies ran while one was open for 3% of the time, Pallas kernels for 0%

profile of v1, /device:TPU:0, one launch (start us, length us, event | category | flops | bytes accessed | tf_op | source)
XLA Modules:
  0.0 407.9 jit_solution(10161963380702721682)
XLA Ops:
  7.2 0.0 copy-start
  7.2 0.0 reduce-scatter.5.cloned.1.call-start
  7.2 2.6 copy.36
  9.8 3.3 fusion
  13.1 0.0 reduce-scatter.5.cloned.1.call-update
  13.1 0.0 all-reduce.3.cloned.1.call-start
  13.1 30.1 %reduce-scatter.5.cloned.1.call-done = f32[4,64,256]{2,1,0:T(8,128)} async-done(((f32[4,256,256]{2,1,0:T(8,128)}), f32[4,64,256]{2,1,0:T(8,128)}) %reduce-scatter.5.cloned.1.call-update) | async-done | bytes 262160 | tf_op jit(solution)/shard_map/reduce_scatter | solution.py:60
  43.2 0.0 all-reduce.3.cloned.1.call-update
  43.3 0.0 reduce-scatter.3.cloned.1.call-start
  43.3 0.0 copy-done
  43.3 7.0 %fusion.6 = f32[2048,1024]{1,0:T(8,128)} fusion(bf16[640,2048]{1,0:T(8,128)(2,1)S(1)} %copy-done, bf16[640,1024]{1,0:T(8,128)(2,1)} %param.12), kind=kOutput, calls=%fused_computation.14 | convolution fusion | flops 2684354560 | bytes 12320768 | tf_op jit(solution)/shard_map/dot_general | solution.py:43
  50.3 0.0 copy-start.4
  50.3 0.0 reduce-scatter.3.cloned.1.call-update
  50.3 0.0 copy-start.6
  50.4 0.0 all-gather.4.cloned.1.call-start
  50.4 37.4 %all-reduce.3.cloned.1.call-done = f32[4,64,256]{2,1,0:T(8,128)} async-done(((f32[4,64,256]{2,1,0:T(8,128)}), f32[4,64,256]{2,1,0:T(8,128)}) %all-reduce.3.cloned.1.call-update) | async-done | bytes 262160 | tf_op jit(solution)/shard_map/psum | solution.py:61
  87.8 0.0 copy-done.4
  87.8 0.0 copy-start.2
  87.8 2.1 fusion.8
  89.9 0.0 all-gather.4.cloned.1.call-update
  89.9 0.0 all-gather.6.cloned.1.call-start
  90.0 144.8 %reduce-scatter.3.cloned.1.call-done = f32[512,1024]{1,0:T(8,128)} async-done(((f32[2048,1024]{1,0:T(8,128)}), f32[512,1024]{1,0:T(8,128)}) %reduce-scatter.3.cloned.1.call-update) | async-done | bytes 2097168 | tf_op jit(solution)/shard_map/reduce_scatter | solution.py:42
  234.8 0.0 all-gather.6.cloned.1.call-update
  234.8 0.0 copy-done.2
  234.8 0.7 multiply_reduce_fusion.3
  235.5 29.9 %all-gather.4.cloned.1.call-done = f32[4,256,256]{2,1,0:T(8,128)} async-done(((f32[4,64,256]{2,1,0:T(8,128)}), f32[4,256,256]{2,1,0:T(8,128)}) %all-gather.4.cloned.1.call-update) | async-done | bytes 1048592 | tf_op jit(solution)/shard_map/all_gather | solution.py:69
  265.4 0.0 copy-done.6
  265.4 2.4 multiply_reduce_fusion.2
  267.8 0.0 copy-start.1
  267.8 86.2 %all-gather.6.cloned.1.call-done = f32[2048,1024]{1,0:T(8,128)} async-done(((f32[512,1024]{1,0:T(8,128)}), f32[2048,1024]{1,0:T(8,128)}) %all-gather.6.cloned.1.call-update) | async-done | bytes 8388624 | tf_op jit(solution)/shard_map/all_gather | solution.py:12
  354.0 5.9 %reduce_sum.45 = f32[512,1024]{1,0:T(8,128)} reduce(f32[4,512,1024]{2,1,0:T(8,128)} %bitcast.24, f32[]{:T(128)} %constant.4.clone.1), dimensions={0}, to_apply=%region_1.0 | reduce | flops 1572864 | bytes 10485764 | tf_op jit(solution)/shard_map/reduce_sum | solution.py:13
  359.9 0.0 copy-start.3
  359.9 2.9 copy.28
  362.8 0.0 copy-done.3
  362.8 4.1 %fusion.7 = f32[4,512,256]{1,2,0:T(8,128)} fusion(f32[512,4,256]{0,2,1:T(8,128)} %bitcast.26, bf16[4,256,256]{2,1,0:T(8,128)(2,1)S(1)} %bitcast.29), kind=kOutput, calls=%fused_computation.15 | convolution fusion | flops 1610612736 | bytes 4718592 | tf_op jit(solution)/shard_map/rbi,bij->rbj/dot_general | solution.py:23
  366.9 2.9 copy.31
  369.8 5.6 %multiply_reduce_fusion = (f32[]{:T(128)}, f32[512,1024]{1,0:T(8,128)}, f32[]{:T(128)}) fusion(f32[512,1024]{1,0:T(8,128)} %copy.31, f32[512,1024]{1,0:T(8,128)} %param.16, f32[512,1024]{1,0:T(8,128)} %reduce_sum.45), kind=kLoop, calls=%fused_computation | loop fusion | flops 3145726 | bytes 8388616 | tf_op jit(solution)/shard_map/reduce_sum | solution.py:77
  375.4 16.8 %all-reduce = (f32[]{:T(128)}, f32[]{:T(128)}, f32[]{:T(128)}, f32[]{:T(128)}) all-reduce(f32[]{:T(128)} %get-tuple-element.22, f32[]{:T(128)} %get-tuple-element.18, f32[]{:T(128)} %multiply_reduce_fusion.3, f32[]{:T(128)} %get-tuple-element.20), channel_id=1, replica_groups=mesh['fs'=4,'rep'=4,'tp'=2] {'fs','tp'}, use_global_device_ids=true, to_apply=%region_3.0 | all-reduce | flops 4 | bytes 32 | tf_op jit(solution)/shard_map/psum | solution.py:74
  395.0 0.0 copy-start.5
  395.0 5.5 %fusion.5 = (bf16[512,1024]{1,0:T(8,128)(2,1)}, f32[512,1024]{1,0:T(8,128)}, f32[512,1024]{1,0:T(8,128)}) fusion(f32[512,1024]{1,0:T(8,128)} %param.15, f32[512,1024]{1,0:T(8,128)} %get-tuple-element.19, f32[]{:T(128)S(6)} %mul.46), kind=kLoop, calls=%fused_computation.13 | loop fusion | flops 1572864 | bytes 9437188 | tf_op jit(solution)/shard_map/convert_element_type | solution.py:93
  400.5 0.0 copy-done.1
  400.5 0.0 copy-done.5
  400.5 0.9 fusion.4
Async XLA Ops:
  7.2 36.1 %copy-start = (bf16[640,2048]{1,0:T(8,128)(2,1)S(1)}, bf16[640,2048]{1,0:T(8,128)(2,1)}, u32[]{:S(2)}) copy-start(bf16[640,2048]{1,0:T(8,128)(2,1)} %param.11) | copy-start | bytes 7864324
  7.2 36.1 %reduce-scatter.5.cloned.1.call-start = ((), (), s32[]{:S(2)}) async-start(), calls=%async_computation.3 | async-start | bytes 1310720 | tf_op jit(solution)/shard_map/reduce_scatter | solution.py:60
  13.1 74.7 %all-reduce.3.cloned.1.call-start = ((), (), s32[]{:S(2)}) async-start(), calls=%async_computation.4 | async-start | bytes 524288 | tf_op jit(solution)/shard_map/psum | solution.py:61
  43.3 191.5 %reduce-scatter.3.cloned.1.call-start = ((), (), s32[]{:S(2)}) async-start(), calls=%async_computation.2 | async-start | bytes 10485760 | tf_op jit(solution)/shard_map/reduce_scatter | solution.py:42
  50.3 37.5 %copy-start.4 = (bf16[4,256,256]{2,1,0:T(8,128)(2,1)S(1)}, bf16[4,256,256]{2,1,0:T(8,128)(2,1)}, u32[]{:S(2)}) copy-start(bf16[4,256,256]{2,1,0:T(8,128)(2,1)} %param.21) | copy-start | bytes 1572868
  50.3 215.1 %copy-start.6 = (bf16[4,64,256]{2,1,0:T(8,128)(2,1)S(1)}, bf16[4,64,256]{2,1,0:T(8,128)(2,1)}, u32[]{:S(2)}) copy-start(bf16[4,64,256]{2,1,0:T(8,128)(2,1)} %param.20) | copy-start | bytes 393220
  50.4 215.1 %all-gather.4.cloned.1.call-start = ((), (), s32[]{:S(2)}) async-start(), calls=%async_computation.5 | async-start | bytes 1310720 | tf_op jit(solution)/shard_map/all_gather | solution.py:69
  87.8 147.0 %copy-start.2 = (f32[4,64,256]{2,1,0:T(8,128)S(1)}, f32[4,64,256]{2,1,0:T(8,128)}, u32[]{:S(2)}) copy-start(f32[4,64,256]{2,1,0:T(8,128)} %all-reduce.3.cloned.1.call-done) | copy-start | bytes 786436
  89.9 264.1 %all-gather.6.cloned.1.call-start = ((), (), s32[]{:S(2)}) async-start(), calls=%async_computation.6 | async-start | bytes 10485760 | tf_op jit(solution)/shard_map/all_gather | solution.py:12
  267.8 132.7 %copy-start.1 = (f32[4,64,256]{2,1,0:T(8,128)}, f32[4,64,256]{2,1,0:T(8,128)S(1)}, u32[]{:S(2)}) copy-start(f32[4,64,256]{2,1,0:T(8,128)S(1)} %get-tuple-element.21) | copy-start | bytes 786436
  359.9 2.9 copy-start.3
  395.0 5.5 %copy-start.5 = (f32[4,64,256]{2,1,0:T(8,128)S(1)}, f32[4,64,256]{2,1,0:T(8,128)}, u32[]{:S(2)}) copy-start(f32[4,64,256]{2,1,0:T(8,128)} %param.18) | copy-start | bytes 786436
Sparse Core Ops, SparseCore 0:
  13.2 29.9 reduce-scatter.4
  46.2 41.5 all-reduce.2
  90.1 144.6 reduce-scatter.2
  236.8 28.5 all-gather.3
  267.1 86.8 all-gather.5
